TPU v7x, 512 devices: a whole 4x4x16 slice. The times are simulated.
512 devices in a mesh: fs: 128 (over z, x, core), tp: 4 (over y).
Axes of the slice: x: 4, y: 4, z: 16, core: 2. Of those that a mesh axis runs over, the one named last changes fastest.
Arguments:
- layer_input: bfloat16 [98304, 2048], P('fs'), may hold values from -6 to 6
- branch_cotangent: bfloat16 [98304, 1024], P('fs', 'tp'), may hold values from -0.014343262 to 0.014343262
- gate_cotangent: bfloat16 [98304, 1024], P('fs', 'tp'), may hold values from -0.014343262 to 0.014343262
- branch_factor: bfloat16 [2048, 128], P('fs'), may hold values from -0.5 to 0.5
- gate_factor: bfloat16 [2048, 128], P('fs'), may hold values from -0.5 to 0.5
- branch_weight: float32 [2048, 1024], P('fs', 'tp'), may hold values from -6 to 6
- gate_weight: float32 [2048, 1024], P('fs', 'tp'), may hold values from -6 to 6
- branch_first: float32 [128, 1024], P(None, 'tp'), may hold values from -6 to 6
- gate_first: float32 [128, 1024], P(None, 'tp'), may hold values from -6 to 6
- branch_second: float32 [128, 1024], P(None, 'tp'), may hold values from 0.0625 to 900
- gate_second: float32 [128, 1024], P(None, 'tp'), may hold values from 0.0625 to 900
Outputs:
- branch_step: float32 [2048, 1024], P('fs', 'tp')
- gate_step: float32 [2048, 1024], P('fs', 'tp')
- branch_new: float32 [2048, 1024], P('fs', 'tp')
- gate_new: float32 [2048, 1024], P('fs', 'tp')
- branch_copy: bfloat16 [2048, 1024], P(None, 'tp')
- gate_copy: bfloat16 [2048, 1024], P(None, 'tp')
- branch_first_new: float32 [128, 1024], P(None, 'tp')
- gate_first_new: float32 [128, 1024], P(None, 'tp')
- branch_second_new: float32 [128, 1024], P(None, 'tp')
- gate_second_new: float32 [128, 1024], P(None, 'tp')
All inputs are finite; a program needn't handle non-finite values.
Results may differ from a plain program's by a relative error of at most 0.00055.
Values may be sent and summed in bfloat16 or wider, within the bound.
No kernel may reach another device: no remote copies, remote signals or barrier semaphores. Data moves between devices by JAX's collectives and lax.ppermute only.
A program may use at most 64 MiB of HBM per device.

v0:
```python
import jax
import jax.numpy as jnp
from jax import lax
from jax.sharding import Mesh
from jax.sharding import PartitionSpec as P

FS = ("fs_0", "fs_1", "fs_2")


first_decay = 0.8
second_decay = 0.9
learn_rate = 0.5


def from_everyone(x, axis):
    copies = jnp.broadcast_to(x, (lax.axis_size(axis), *x.shape))
    return lax.all_to_all(copies, axis, split_axis=0, concat_axis=0, tiled=True)


def laid_out(blocks, dim):
    shape = list(blocks.shape[1:])
    shape[dim] *= blocks.shape[0]
    return jnp.moveaxis(blocks, 0, dim).reshape(shape)


def gathered_by_axis(x, axes, dim):
    far, near = axes
    blocks = from_everyone(from_everyone(x, far), near)
    return laid_out(blocks.swapaxes(0, 1).reshape(-1, *x.shape), dim)


def in_one_piece(arrays, axis, dim, along):
    both = jnp.concatenate(arrays, axis=along)
    result, at, gathered = (gathered_by_axis(both, axis, dim), 0, [])
    for a in arrays:
        gathered.append(lax.slice_in_dim(result, at, at + a.shape[along], axis=along))
        at += a.shape[along]
    return tuple(gathered)


def padded_to(lines, peers):
    spare = -len(lines) % peers
    return jnp.pad(lines, [(0, spare)] + [(0, 0)] * (lines.ndim - 1))


def split_up(x, dim, peers):
    shape = x.shape
    blocks = x.reshape(*shape[:dim], peers, shape[dim] // peers, *shape[dim + 1 :])
    return jnp.moveaxis(blocks, dim, 0)


def summed_on_arrival(x, axis, dim):
    peers = lax.axis_size(axis)
    blocks = lax.all_to_all(split_up(x, dim, peers), axis, 0, 0, tiled=True)
    return jnp.sum(blocks, axis=0)


def sum_in_two_steps(x, axes, dim):
    far, near = axes
    blocks = split_up(x, dim, lax.axis_size(far))
    nearer = summed_on_arrival(blocks, near, dim + 1)
    arrived = lax.all_to_all(nearer, far, split_axis=0, concat_axis=0, tiled=True)
    return arrived.sum(axis=0)


def sum_by_parts(x, axes):
    padded = padded_to(x, lax.axis_size(axes[0]) * lax.axis_size(axes[1]))
    whole = gathered_by_axis(sum_in_two_steps(padded, axes, 0), axes, 0)
    return lax.slice_in_dim(whole, 0, len(x)).reshape(x.shape)


def packed_total(arrays, axis):
    flat, at, gathered = (jnp.concatenate([a.reshape(-1) for a in arrays]), 0, [])
    total = sum_by_parts(flat, axis)
    for a in arrays:
        gathered.append(total[at : at + a.size].reshape(a.shape))
        at += a.size
    return tuple(gathered)


def taken_together(x, axis):
    everything = from_everyone(x, axis)
    return jnp.sum(everything, axis=0)


def update_moments(projected, first_old, second_old):
    first_new = first_decay * first_old + (1.0 - first_decay) * projected
    second_new = second_decay * second_old + (1.0 - second_decay) * projected * projected
    return (first_new, second_new, first_new / jnp.sqrt(second_new))


def local(
    layer_input,
    branch_cotangent,
    gate_cotangent,
    branch_factor,
    gate_factor,
    branch_weight,
    gate_weight,
    branch_first,
    gate_first,
    branch_second,
    gate_second,
):
    highest = lax.Precision.HIGHEST
    width = branch_cotangent.shape[1]
    branch_whole, gate_whole = in_one_piece(
        (branch_factor, gate_factor), (("fs_0", "fs_1"), "fs_2"), 0, 1
    )
    branch_rows = jnp.dot(layer_input, branch_whole, preferred_element_type=jnp.float32)
    gate_rows = jnp.dot(layer_input, gate_whole, preferred_element_type=jnp.float32)
    branch_local = jnp.einsum(
        "tr,tw->rw", branch_rows, branch_cotangent.astype(jnp.float32), precision=highest
    )
    gate_local = jnp.einsum(
        "tr,tw->rw", gate_rows, gate_cotangent.astype(jnp.float32), precision=highest
    )
    branch_projected, gate_projected = packed_total(
        (branch_local, gate_local), (("fs_0", "fs_1"), "fs_2")
    )
    branch_first_new, branch_second_new, branch_direction = update_moments(
        branch_projected, branch_first, branch_second
    )
    gate_first_new, gate_second_new, gate_direction = update_moments(
        gate_projected, gate_first, gate_second
    )
    local_squares = jnp.sum(branch_direction * branch_direction) + jnp.sum(
        gate_direction * gate_direction
    )
    sum_squares = taken_together(local_squares, "tp")
    entries = 2 * branch_direction.shape[0] * width * lax.axis_size("tp")
    step_scale = learn_rate / jnp.sqrt(sum_squares / entries + 1e-06)
    branch_step = -step_scale * jnp.dot(
        branch_factor.astype(jnp.float32), branch_direction, precision=highest
    )
    gate_step = -step_scale * jnp.dot(
        gate_factor.astype(jnp.float32), gate_direction, precision=highest
    )
    branch_new = branch_weight + branch_step
    gate_new = gate_weight + gate_step
    branch_copy, gate_copy = in_one_piece(
        (branch_new.astype(jnp.bfloat16), gate_new.astype(jnp.bfloat16)),
        (("fs_0", "fs_1"), "fs_2"),
        0,
        1,
    )
    return (
        branch_step,
        gate_step,
        branch_new,
        gate_new,
        branch_copy,
        gate_copy,
        branch_first_new,
        gate_first_new,
        branch_second_new,
        gate_second_new,
    )


def solution(mesh):
    finer = Mesh(mesh.devices.reshape(16, 4, 2, mesh.shape["tp"]), ("fs_0", "fs_1", "fs_2", "tp"))
    in_specs = (
        P(FS, None),
        P(FS, "tp"),
        P(FS, "tp"),
        P(FS, None),
        P(FS, None),
        P(FS, "tp"),
        P(FS, "tp"),
        P(None, "tp"),
        P(None, "tp"),
        P(None, "tp"),
        P(None, "tp"),
    )
    out_specs = (
        P(FS, "tp"),
        P(FS, "tp"),
        P(FS, "tp"),
        P(FS, "tp"),
        P(None, "tp"),
        P(None, "tp"),
        P(None, "tp"),
        P(None, "tp"),
        P(None, "tp"),
        P(None, "tp"),
    )
    return jax.shard_map(local, mesh=finer, in_specs=in_specs, out_specs=out_specs, check_vma=False)
```

profile of v0, /device:TPU:1, one launch (start us, length us, event | category | flops | bytes accessed | tf_op | source)
XLA Modules:
  0.0 207.9 jit_solution(2880932666247326444)
XLA Ops:
  0.7 0.9 pad_maximum_fusion.1
  1.6 50.0 %all_to_all.54 = bf16[64,16,256]{2,1,0:T(8,128)(2,1)S(1)} all-to-all(bf16[64,16,256]{2,1,0:T(8,128)(2,1)S(1)} %broadcast_in_dim.21), channel_id=1, replica_groups=mesh['fs_0'=16,'fs_1'=4,'fs_2'=2,'tp'=4] {'fs_0','fs_1'}, dimensions={0} | all-to-all | bytes 1048576 | tf_op jit(solution)/shard_map/all_to_all | solution.py:17
  51.6 7.0 %all_to_all.55 = bf16[2,64,16,256]{3,2,1,0:T(8,128)(2,1)S(1)} all-to-all(bf16[2,64,16,256]{3,2,1,0:T(8,128)(2,1)S(1)} %broadcast_in_dim.22), channel_id=1, replica_groups=mesh['fs_0'=16,'fs_1'=4,'fs_2'=2,'tp'=4] {'fs_2'}, dimensions={0} | all-to-all | bytes 2097152 | tf_op jit(solution)/shard_map/all_to_all | solution.py:17
  58.8 1.2 fusion.2
  60.0 1.2 fusion.4
  61.2 1.0 fusion.15
  62.2 1.6 concatenate.16
  63.9 1.6 copy.38
  65.4 2.0 fusion.14
  67.4 1.0 concatenate.15
  68.5 0.9 maximum_bitcast_fusion
  69.4 4.0 %all_to_all.56 = f32[2,64,512]{2,1,0:T(8,128)S(1)} all-to-all(f32[2,64,512]{2,1,0:T(8,128)S(1)} %maximum_bitcast_fusion), channel_id=1, replica_groups=mesh['fs_0'=16,'fs_1'=4,'fs_2'=2,'tp'=4] {'fs_2'}, dimensions={0} | all-to-all | bytes 524288 | tf_op jit(solution)/shard_map/all_to_all | solution.py:54
  73.5 20.6 %all_to_all.57 = f32[64,1,512]{2,1,0:T(1,128)S(1)} all-to-all(f32[64,1,512]{2,1,0:T(1,128)S(1)} %all_to_all.37), channel_id=1, replica_groups=mesh['fs_0'=16,'fs_1'=4,'fs_2'=2,'tp'=4] {'fs_0','fs_1'}, dimensions={0} | all-to-all | bytes 262144 | tf_op jit(solution)/shard_map/all_to_all | solution.py:62
  94.2 21.3 %all_to_all.58 = f32[64,1,512]{2,1,0:T(1,128)S(1)} all-to-all(f32[64,1,512]{2,1,0:T(1,128)S(1)} %broadcast_in_dim.23), channel_id=1, replica_groups=mesh['fs_0'=16,'fs_1'=4,'fs_2'=2,'tp'=4] {'fs_0','fs_1'}, dimensions={0} | all-to-all | bytes 262144 | tf_op jit(solution)/shard_map/all_to_all | solution.py:17
  115.6 6.8 %all_to_all.59 = f32[2,64,512]{2,1,0:T(8,128)S(1)} all-to-all(f32[2,64,512]{2,1,0:T(8,128)S(1)} %broadcast_in_dim.24), channel_id=1, replica_groups=mesh['fs_0'=16,'fs_1'=4,'fs_2'=2,'tp'=4] {'fs_2'}, dimensions={0} | all-to-all | bytes 524288 | tf_op jit(solution)/shard_map/all_to_all | solution.py:17
  122.5 0.8 reshape.45
  123.3 0.8 reshape.44
  124.1 2.5 %multiply_reduce_fusion = (f32[]{:T(128)}, f32[128,256]{1,0:T(8,128)S(1)}, f32[128,256]{1,0:T(8,128)S(1)}, f32[]{:T(128)}, f32[128,256]{1,0:T(8,128)S(1)}, /*index=5*/f32[128,256]{1,0:T(8,128)}) fusion(f32[128,256]{1,0:T(8,128)} %reshape.45, f32[128,256]{1,0:T(8,128)} %param.21, f32[128,256]{1,0:T(8,128)} %param.19, f32[128,256]{1,0:T(8,128)} %reshape.44, ...), kind=kLoop, calls=%fused_computation.14 | loop fusion | flops 655358 | bytes 1310728 | tf_op jit(solution)/shard_map/reduce_sum | solution.py:127
  128.0 8.1 %all_to_all.60 = f32[4,1,1]{2,1,0:T(1,128)S(1)} all-to-all(f32[4,1,1]{2,1,0:T(1,128)S(1)} %broadcast_in_dim.25), channel_id=1, replica_groups=mesh['fs_0'=16,'fs_1'=4,'fs_2'=2,'tp'=4] {'tp'}, dimensions={0} | all-to-all | bytes 32 | tf_op jit(solution)/shard_map/all_to_all | solution.py:17
  137.4 1.5 fusion.9
  138.9 1.7 fusion.8
  140.7 55.4 %all_to_all.61 = bf16[64,16,512]{2,1,0:T(8,128)(2,1)S(1)} all-to-all(bf16[64,16,512]{2,1,0:T(8,128)(2,1)S(1)} %broadcast_in_dim.26), channel_id=1, replica_groups=mesh['fs_0'=16,'fs_1'=4,'fs_2'=2,'tp'=4] {'fs_0','fs_1'}, dimensions={0} | all-to-all | bytes 2097152 | tf_op jit(solution)/shard_map/all_to_all | solution.py:17
  196.5 9.7 %all_to_all.62 = bf16[2,64,16,512]{3,2,1,0:T(8,128)(2,1)S(1)} all-to-all(bf16[2,64,16,512]{3,2,1,0:T(8,128)(2,1)S(1)} %broadcast_in_dim.27), channel_id=1, replica_groups=mesh['fs_0'=16,'fs_1'=4,'fs_2'=2,'tp'=4] {'fs_2'}, dimensions={0} | all-to-all | bytes 4194304 | tf_op jit(solution)/shard_map/all_to_all | solution.py:17
  206.4 1.5 fusion.12
  (33 shorter events, 2.1 us)
Async XLA Ops:
  0.6 58.1 %copy-start = (bf16[768,2048]{1,0:T(8,128)(2,1)S(1)}, bf16[768,2048]{1,0:T(8,128)(2,1)}, u32[]{:S(2)}) copy-start(bf16[768,2048]{1,0:T(8,128)(2,1)} %param.11) | copy-start | bytes 9437188
  58.8 2.4 %copy-start.4 = (bf16[768,256]{1,0:T(8,128)(2,1)S(1)}, bf16[768,256]{1,0:T(8,128)(2,1)}, u32[]{:S(2)}) copy-start(bf16[768,256]{1,0:T(8,128)(2,1)} %param.13) | copy-start | bytes 1179652
  69.4 68.0 %copy-start.5 = (bf16[16,128]{1,0:T(8,128)(2,1)S(1)}, bf16[16,128]{1,0:T(8,128)(2,1)}, u32[]{:S(2)}) copy-start(bf16[16,128]{1,0:T(8,128)(2,1)} %param.15) | copy-start | bytes 12292
  69.4 69.5 %copy-start.6 = (bf16[16,128]{1,0:T(8,128)(2,1)S(1)}, bf16[16,128]{1,0:T(8,128)(2,1)}, u32[]{:S(2)}) copy-start(bf16[16,128]{1,0:T(8,128)(2,1)} %param.14) | copy-start | bytes 12292
  126.6 69.8 %copy-start.1 = (f32[128,256]{1,0:T(8,128)}, f32[128,256]{1,0:T(8,128)S(1)}, u32[]{:S(2)}) copy-start(f32[128,256]{1,0:T(8,128)S(1)} %get-tuple-element.15) | copy-start | bytes 393220
  126.6 69.8 %copy-start.2 = (f32[128,256]{1,0:T(8,128)}, f32[128,256]{1,0:T(8,128)S(1)}, u32[]{:S(2)}) copy-start(f32[128,256]{1,0:T(8,128)S(1)} %get-tuple-element.16) | copy-start | bytes 393220
  126.6 69.8 %copy-start.3 = (f32[128,256]{1,0:T(8,128)}, f32[128,256]{1,0:T(8,128)S(1)}, u32[]{:S(2)}) copy-start(f32[128,256]{1,0:T(8,128)S(1)} %get-tuple-element.27) | copy-start | bytes 393220
where the time goes:
time: 209 us; the launch traced here: 208 us
  blocking collectives  183 us (88%)
  matrix products  8.59 us (4%)
  local copies, waits for them, and re-layouts  8.54 us (4%)
  other arithmetic  5.08 us (2%)
  between operations  2.84 us (1%)
    all_to_all x7, blocking collectives, from_everyone(): return lax.all_to_all(copies, axis, split_axis=0, concat_axis=0, tiled=True)  158 us
    all_to_all x1, blocking collectives, sum_in_two_steps(): lax.all_to_all(nearer, far, split_axis=0, concat_axis=0, tiled=True)  20.6 us
    concatenate x4, local copies, waits for them, and re-layouts, packed_total(): jnp.concatenate([a.reshape(-1) for a in arrays])  4.24 us

commit v1 on v0

v1 whole, which is shorter than its diff:
```python
import jax
import jax.numpy as jnp
from jax import lax
from jax.sharding import Mesh
from jax.sharding import PartitionSpec as P

FS = ("zh", "zl", "x", "c")
Z = ("zh", "zl")

first_decay = 0.8
second_decay = 0.9
learn_rate = 0.5


def exchanged(blocks, axes):
    return lax.all_to_all(blocks, axes, split_axis=0, concat_axis=0, tiled=True)


def from_everyone(x, axes):
    peers = 1
    for a in axes:
        peers *= lax.axis_size(a)
    return exchanged(jnp.broadcast_to(x, (peers, *x.shape)), axes)


def whole_factors(branch_factor, gate_factor):
    rows, rank = branch_factor.shape
    half = rows // 2
    quarters = jnp.stack(
        [branch_factor[:half], branch_factor[half:], gate_factor[:half], gate_factor[half:]]
    )
    mine = lax.dynamic_index_in_dim(quarters, lax.axis_index("tp"), 0, keepdims=False)
    along_z = from_everyone(mine, Z)
    along_plane = from_everyone(along_z, ("x", "tp"))
    both = from_everyone(along_plane, ("c",))
    nz = along_z.shape[0]
    nx = lax.axis_size("x")
    parts = both.reshape(2, nx, 2, 2, nz, half, rank)
    return parts.transpose(4, 1, 0, 3, 5, 2, 6).reshape(nz * nx * 2 * rows, 2 * rank)


def two_parts(x):
    high = lax.reduce_precision(x, 8, 7)
    return high.astype(jnp.bfloat16), (x - high).astype(jnp.bfloat16)


def projected_locally(rows, cotangent):
    high, low = two_parts(rows)
    rank = rows.shape[1]
    both = lax.dot_general(
        jnp.concatenate([high, low], axis=1),
        cotangent,
        (((0,), (0,)), ((), ())),
        preferred_element_type=jnp.float32,
    )
    return both[:rank] + both[rank:]


def summed_over_fs(branch_local, gate_local):
    mine = exchanged(jnp.stack([branch_local, gate_local]), ("c",)).sum(axis=0)
    rank, width = mine.shape
    near = lax.axis_size("zl") * lax.axis_size("x")
    piece = exchanged(mine.reshape(near, rank // near, width), ("zl", "x")).sum(axis=0)
    total = from_everyone(piece, ("zh",)).sum(axis=0)
    whole = from_everyone(total, ("zl", "x")).reshape(rank, width)
    both = from_everyone(whole, ("c",))
    return both[0], both[1]


def update_moments(projected, first_old, second_old):
    first_new = first_decay * first_old + (1.0 - first_decay) * projected
    second_new = second_decay * second_old + (1.0 - second_decay) * projected * projected
    return (first_new, second_new, first_new / jnp.sqrt(second_new))


def times_direction(factor, direction):
    high = lax.reduce_precision(direction, 8, 7)
    rest = direction - high
    middle = lax.reduce_precision(rest, 8, 7)
    low = rest - middle
    width = direction.shape[1]
    parts = jnp.concatenate([p.astype(jnp.bfloat16) for p in (high, middle, low)], axis=1)
    out = jnp.dot(factor, parts, preferred_element_type=jnp.float32)
    return out[:, :width] + (out[:, width : 2 * width] + out[:, 2 * width :])


def whole_copies(branch_new, gate_new):
    mine = jnp.concatenate([branch_new, gate_new], axis=1).astype(jnp.bfloat16)
    rows, width = mine.shape
    along_z = from_everyone(mine, Z)
    along_x = from_everyone(along_z, ("x",))
    both = from_everyone(along_x, ("c",))
    whole = both.transpose(2, 1, 0, 3, 4).reshape(-1, width)
    return whole[:, : width // 2], whole[:, width // 2 :]


def local(
    layer_input,
    branch_cotangent,
    gate_cotangent,
    branch_factor,
    gate_factor,
    branch_weight,
    gate_weight,
    branch_first,
    gate_first,
    branch_second,
    gate_second,
):
    rank, width = branch_first.shape
    factors = whole_factors(branch_factor, gate_factor)
    rows = jnp.dot(layer_input, factors, preferred_element_type=jnp.float32)
    branch_local = projected_locally(rows[:, :rank], branch_cotangent)
    gate_local = projected_locally(rows[:, rank:], gate_cotangent)
    branch_projected, gate_projected = summed_over_fs(branch_local, gate_local)
    branch_first_new, branch_second_new, branch_direction = update_moments(
        branch_projected, branch_first, branch_second
    )
    gate_first_new, gate_second_new, gate_direction = update_moments(
        gate_projected, gate_first, gate_second
    )
    local_squares = jnp.sum(branch_direction * branch_direction) + jnp.sum(
        gate_direction * gate_direction
    )
    squares = from_everyone(jnp.full((1, 128), local_squares), ("tp",))
    sum_squares = jnp.sum(squares, axis=0)[0, 0]
    entries = 2 * rank * width * lax.axis_size("tp")
    step_scale = learn_rate / jnp.sqrt(sum_squares / entries + 1e-06)
    branch_step = -step_scale * times_direction(branch_factor, branch_direction)
    gate_step = -step_scale * times_direction(gate_factor, gate_direction)
    branch_new = branch_weight + branch_step
    gate_new = gate_weight + gate_step
    branch_copy, gate_copy = whole_copies(branch_new, gate_new)
    return (
        branch_step,
        gate_step,
        branch_new,
        gate_new,
        branch_copy,
        gate_copy,
        branch_first_new,
        gate_first_new,
        branch_second_new,
        gate_second_new,
    )


def solution(mesh):
    finer = Mesh(
        mesh.devices.reshape(8, 2, 4, 2, mesh.shape["tp"]), ("zh", "zl", "x", "c", "tp")
    )
    sharded = P(FS, None)
    split = P(FS, "tp")
    kept = P(None, "tp")
    in_specs = (sharded, split, split, sharded, sharded, split, split, kept, kept, kept, kept)
    out_specs = (split, split, split, split, kept, kept, kept, kept, kept, kept)
    return jax.shard_map(local, mesh=finer, in_specs=in_specs, out_specs=out_specs, check_vma=False)
```

time: 209 us -> 158 us (0.76)
  blocking collectives: 183 us -> 135 us
  matrix products: 8.59 us -> 1.91 us
  local copies, waits for them, and re-layouts: 8.54 us -> 4.43 us
  waiting for transfers between devices: 0 us -> 3.68 us
  starting transfers between devices: 0 us -> 3.22 us
    all_to_all x9 -> x11, blocking collectives: 183 us -> 135 us  [exchanged(): return lax.all_to_all(blocks, axes, split_axis=0, concat_axis=0, tiled=True)]
    dot_general x6 -> x5, matrix products: 8.59 us -> 1.91 us  [the longest x1 1.08 us: local(): rows = jnp.dot(layer_input, factors, preferred_element_type=jnp.float32)]
    concatenate x4 -> x0, local copies, waits for them, and re-layouts: 4.24 us -> none  [packed_total(): jnp.concatenate([a.reshape(-1) for a in arrays])]
    all_to_all x0 -> x1, waiting for transfers between devices: none -> 3.68 us  [exchanged(): return lax.all_to_all(blocks, axes, split_axis=0, concat_axis=0, tiled=True)]
    convert_element_type x0 -> x4, other arithmetic: none -> 3.28 us  [the longest x3 3.18 us: times_direction(): p.astype(jnp.bfloat16)]
    reduce_sum x4, other arithmetic: 3.29 us -> 0.06 us  [the longest x1 0.02 us: local(): sum_squares = jnp.sum(squares, axis=0)[0, 0]]
    all_to_all x0 -> x1, starting transfers between devices: none -> 3.22 us  [exchanged(): return lax.all_to_all(blocks, axes, split_axis=0, concat_axis=0, tiled=True)]
  transfers between devices with their start and end apart: 0 -> 1, of which waited for: 0 -> 1; matrix products, arithmetic and copies ran while one was open for 0% -> 0% of each run, Pallas kernels for 0% -> 0%
where the time goes in v1:
time: 158 us; the launch traced here: 155 us
  blocking collectives  135 us (85%)
  other arithmetic  4.65 us (3%)
  local copies, waits for them, and re-layouts  4.43 us (3%)
  waiting for transfers between devices  3.68 us (2%)
  starting transfers between devices  3.22 us (2%)
  between operations  2.31 us (1%)
  matrix products  1.91 us (1%)
    all_to_all x11, blocking collectives, exchanged(): return lax.all_to_all(blocks, axes, split_axis=0, concat_axis=0, tiled=True)  135 us
    all_to_all x1, waiting for transfers between devices, exchanged(): return lax.all_to_all(blocks, axes, split_axis=0, concat_axis=0, tiled=True)  3.68 us
    all_to_all x1, starting transfers between devices, exchanged(): return lax.all_to_all(blocks, axes, split_axis=0, concat_axis=0, tiled=True)  3.22 us
    convert_element_type x3, other arithmetic, times_direction(): p.astype(jnp.bfloat16)  3.18 us
  transfers between devices with their start and end apart: 1, of which 1 were waited for; matrix products, arithmetic and copies ran while one was open for 0% of the time, Pallas kernels for 0%

profile of v1, /device:TPU:1, one launch (start us, length us, event | category | flops | bytes accessed | tf_op | source)
XLA Modules:
  0.0 155.4 jit_solution(11984082673532972364)
XLA Ops:
  0.7 0.9 slice_bitcast_fusion.2
  1.6 27.1 %all_to_all.60 = bf16[16,8,128]{2,1,0:T(8,128)(2,1)S(1)} all-to-all(bf16[16,8,128]{2,1,0:T(8,128)(2,1)S(1)} %broadcast_in_dim.27), channel_id=1, replica_groups=mesh['zh'=8,'zl'=2,'x'=4,'c'=2,'tp'=4] {'zh','zl'}, dimensions={0} | all-to-all | bytes 65536 | tf_op jit(solution)/shard_map/all_to_all | solution.py:16
  28.8 15.8 %all_to_all.61 = bf16[16,16,8,128]{3,2,1,0:T(8,128)(2,1)S(1)} all-to-all(bf16[16,16,8,128]{3,2,1,0:T(8,128)(2,1)S(1)} %broadcast_in_dim.28), channel_id=1, replica_groups=mesh['zh'=8,'zl'=2,'x'=4,'c'=2,'tp'=4] {'x','tp'}, dimensions={0} | all-to-all | bytes 1048576 | tf_op jit(solution)/shard_map/all_to_all | solution.py:16
  44.6 0.3 broadcast_in_dim.29
  44.9 7.5 %all_to_all.62 = bf16[2,16,16,8,128]{4,3,2,1,0:T(8,128)(2,1)S(1)} all-to-all(bf16[2,16,16,8,128]{4,3,2,1,0:T(8,128)(2,1)S(1)} %broadcast_in_dim.29), channel_id=1, replica_groups=mesh['zh'=8,'zl'=2,'x'=4,'c'=2,'tp'=4] {'c'}, dimensions={0} | all-to-all | bytes 2097152 | tf_op jit(solution)/shard_map/all_to_all | solution.py:16
  52.3 0.3 copy.30
  52.7 1.1 convolution_bitcast_fusion
  54.5 4.0 %all_to_all.63 = f32[2,128,256]{2,1,0:T(8,128)S(1)} all-to-all(f32[2,128,256]{2,1,0:T(8,128)S(1)} %pad_maximum_fusion), channel_id=1, replica_groups=mesh['zh'=8,'zl'=2,'x'=4,'c'=2,'tp'=4] {'c'}, dimensions={0} | all-to-all | bytes 524288 | tf_op jit(solution)/shard_map/all_to_all | solution.py:16
  58.5 8.0 %all_to_all.64 = f32[8,16,256]{2,1,0:T(8,128)S(1)} all-to-all(f32[8,16,256]{2,1,0:T(8,128)S(1)} %bitcast.59), channel_id=1, replica_groups=mesh['zh'=8,'zl'=2,'x'=4,'c'=2,'tp'=4] {'zl','x'}, dimensions={0} | all-to-all | bytes 262144 | tf_op jit(solution)/shard_map/all_to_all | solution.py:16
  66.6 15.3 %all_to_all.65 = f32[8,16,256]{2,1,0:T(8,128)S(1)} all-to-all(f32[8,16,256]{2,1,0:T(8,128)S(1)} %broadcast_in_dim.30), channel_id=1, replica_groups=mesh['zh'=8,'zl'=2,'x'=4,'c'=2,'tp'=4] {'zh'}, dimensions={0} | all-to-all | bytes 262144 | tf_op jit(solution)/shard_map/all_to_all | solution.py:16
  81.9 7.8 %all_to_all.66 = f32[8,16,256]{2,1,0:T(8,128)S(1)} all-to-all(f32[8,16,256]{2,1,0:T(8,128)S(1)} %broadcast_in_dim.31), channel_id=1, replica_groups=mesh['zh'=8,'zl'=2,'x'=4,'c'=2,'tp'=4] {'zl','x'}, dimensions={0} | all-to-all | bytes 262144 | tf_op jit(solution)/shard_map/all_to_all | solution.py:16
  89.8 8.9 %all_to_all.67 = f32[2,128,256]{2,1,0:T(8,128)S(1)} all-to-all(f32[2,128,256]{2,1,0:T(8,128)S(1)} %broadcast_in_dim.32), channel_id=1, replica_groups=mesh['zh'=8,'zl'=2,'x'=4,'c'=2,'tp'=4] {'c'}, dimensions={0} | all-to-all | bytes 524288 | tf_op jit(solution)/shard_map/all_to_all | solution.py:16
  98.7 2.5 %reduce-precision_convert_fusion.3 = (bf16[128,256]{1,0:T(8,128)(2,1)S(1)}, f32[128,256]{1,0:T(8,128)S(1)}, f32[128,256]{1,0:T(8,128)}, f32[128,256]{1,0:T(8,128...) fusion(f32[2,128,256]{2,1,0:T(8,128)S(1)} %all_to_all.67, ...), kind=kLoop, calls=%fused_computation.33 | loop fusion | flops 655359 | bytes 1638404 | tf_op jit(solution)/shard_map/convert_element_type | solution.py:82
  101.2 0.6 reduce-precision_convert_fusion.2
  103.2 0.6 broadcast_in_dim_broadcast_in_dim.3
  103.7 3.2 %all-to-all-start.8 = ((f32[4,1,128]{2,1,0:T(1,128)}), f32[4,1,128]{2,1,0:T(1,128)S(1)}, u32[]{:S(2)}, u32[]{:S(2)}) async-start(f32[4,1,128]{2,1,0:T(1,128)} %broadcast_in_dim_broadcast_in_dim.3), calls=%async_computation.8 | async-start | bytes 4096 | tf_op jit(solution)/shard_map/all_to_all | solution.py:16
  107.3 3.7 %all-to-all-done.8 = f32[4,1,128]{2,1,0:T(1,128)S(1)} async-done(((f32[4,1,128]{2,1,0:T(1,128)}), f32[4,1,128]{2,1,0:T(1,128)S(1)}, u32[]{:S(2)}, u32[]{:S(2)}) %all-to-all-start.8) | async-done | bytes 2080 | tf_op jit(solution)/shard_map/all_to_all | solution.py:16
  111.1 0.6 fusion.40
  111.7 0.6 fusion.38
  112.4 15.3 %all_to_all.68 = bf16[16,16,512]{2,1,0:T(8,128)(2,1)S(1)} all-to-all(bf16[16,16,512]{2,1,0:T(8,128)(2,1)S(1)} %broadcast_in_dim.33), channel_id=1, replica_groups=mesh['zh'=8,'zl'=2,'x'=4,'c'=2,'tp'=4] {'zh','zl'}, dimensions={0} | all-to-all | bytes 524288 | tf_op jit(solution)/shard_map/all_to_all | solution.py:16
  127.9 12.2 %all_to_all.69 = bf16[4,16,16,512]{3,2,1,0:T(8,128)(2,1)S(1)} all-to-all(bf16[4,16,16,512]{3,2,1,0:T(8,128)(2,1)S(1)} %broadcast_in_dim.34), channel_id=1, replica_groups=mesh['zh'=8,'zl'=2,'x'=4,'c'=2,'tp'=4] {'x'}, dimensions={0} | all-to-all | bytes 2097152 | tf_op jit(solution)/shard_map/all_to_all | solution.py:16
  140.1 0.3 broadcast_in_dim.35
  140.4 13.3 %all_to_all.70 = bf16[2,4,16,16,512]{4,3,1,2,0:T(8,128)(2,1)S(1)} all-to-all(bf16[2,4,16,16,512]{4,3,1,2,0:T(8,128)(2,1)S(1)} %broadcast_in_dim.35), channel_id=1, replica_groups=mesh['zh'=8,'zl'=2,'x'=4,'c'=2,'tp'=4] {'c'}, dimensions={0} | all-to-all | bytes 4194304 | tf_op jit(solution)/shard_map/all_to_all | solution.py:16
  154.0 1.5 fusion.44
  (38 shorter events, 1.7 us)
Async XLA Ops:
  0.6 52.0 %copy-start = (bf16[768,2048]{1,0:T(8,128)(2,1)S(1)}, bf16[768,2048]{1,0:T(8,128)(2,1)}, u32[]{:S(2)}) copy-start(bf16[768,2048]{1,0:T(8,128)(2,1)} %param.11) | copy-start | bytes 9437188
  52.6 1.2 copy-start.5
  52.6 1.5 copy-start.6
  54.5 56.6 %copy-start.1 = (f32[16,256]{1,0:T(8,128)S(1)}, f32[16,256]{1,0:T(8,128)}, u32[]{:S(2)}) copy-start(f32[16,256]{1,0:T(8,128)} %param.17) | copy-start | bytes 49156
  58.5 48.5 %copy-start.3 = (bf16[16,128]{1,0:T(8,128)(2,1)S(1)}, bf16[16,128]{1,0:T(8,128)(2,1)}, u32[]{:S(2)}) copy-start(bf16[16,128]{1,0:T(8,128)(2,1)} %param.15) | copy-start | bytes 12292
  58.5 48.7 %copy-start.4 = (bf16[16,128]{1,0:T(8,128)(2,1)S(1)}, bf16[16,128]{1,0:T(8,128)(2,1)}, u32[]{:S(2)}) copy-start(bf16[16,128]{1,0:T(8,128)(2,1)} %param.14) | copy-start | bytes 12292
  58.5 53.2 %copy-start.2 = (f32[16,256]{1,0:T(8,128)S(1)}, f32[16,256]{1,0:T(8,128)}, u32[]{:S(2)}) copy-start(f32[16,256]{1,0:T(8,128)} %param.16) | copy-start | bytes 49156
  103.7 7.3 %all-to-all-start.8 = ((f32[4,1,128]{2,1,0:T(1,128)}), f32[4,1,128]{2,1,0:T(1,128)S(1)}, u32[]{:S(2)}, u32[]{:S(2)}) async-start(f32[4,1,128]{2,1,0:T(1,128)} %broadcast_in_dim_broadcast_in_dim.3), calls=%async_computation.8 | async-start | bytes 4096 | tf_op jit(solution)/shard_map/all_to_all | solution.py:16

commit v2 on v1

--- a/solution.py
+++ b/solution.py
@@ -5,7 +5,6 @@
 from jax.sharding import PartitionSpec as P
 
 FS = ("zh", "zl", "x", "c")
-Z = ("zh", "zl")
 
 first_decay = 0.8
 second_decay = 0.9
@@ -23,20 +22,20 @@
     return exchanged(jnp.broadcast_to(x, (peers, *x.shape)), axes)
 
 
-def whole_factors(branch_factor, gate_factor):
-    rows, rank = branch_factor.shape
-    half = rows // 2
-    quarters = jnp.stack(
-        [branch_factor[:half], branch_factor[half:], gate_factor[:half], gate_factor[half:]]
-    )
-    mine = lax.dynamic_index_in_dim(quarters, lax.axis_index("tp"), 0, keepdims=False)
-    along_z = from_everyone(mine, Z)
-    along_plane = from_everyone(along_z, ("x", "tp"))
-    both = from_everyone(along_plane, ("c",))
-    nz = along_z.shape[0]
-    nx = lax.axis_size("x")
-    parts = both.reshape(2, nx, 2, 2, nz, half, rank)
-    return parts.transpose(4, 1, 0, 3, 5, 2, 6).reshape(nz * nx * 2 * rows, 2 * rank)
+NEAR = ("zl", "x")
+
+
+def gathered(block):
+    along_far = from_everyone(block, ("zh",))
+    along_near = from_everyone(along_far, NEAR)
+    mine = along_near.reshape(lax.axis_size("zl"), lax.axis_size("x"), *along_far.shape)
+    other = lax.ppermute(mine, "c", [(0, 1), (1, 0)])
+    core = lax.axis_index("c")
+    return jnp.stack([jnp.where(core == 0, mine, other), jnp.where(core == 0, other, mine)])
+
+
+def in_row_order(blocks):
+    return blocks.transpose(3, 1, 2, 0, 4, 5).reshape(-1, blocks.shape[-1])
 
 
 def two_parts(x):
@@ -57,14 +56,14 @@
 
 
 def summed_over_fs(branch_local, gate_local):
-    mine = exchanged(jnp.stack([branch_local, gate_local]), ("c",)).sum(axis=0)
-    rank, width = mine.shape
-    near = lax.axis_size("zl") * lax.axis_size("x")
-    piece = exchanged(mine.reshape(near, rank // near, width), ("zl", "x")).sum(axis=0)
+    both = jnp.stack([branch_local, gate_local])
+    group = ("zl", "x", "c")
+    peers = lax.axis_size("zl") * lax.axis_size("x") * lax.axis_size("c")
+    pieces = both.reshape(peers, -1, both.shape[-1])
+    piece = exchanged(pieces, group).sum(axis=0)
     total = from_everyone(piece, ("zh",)).sum(axis=0)
-    whole = from_everyone(total, ("zl", "x")).reshape(rank, width)
-    both = from_everyone(whole, ("c",))
-    return both[0], both[1]
+    whole = from_everyone(total, group).reshape(both.shape)
+    return whole[0], whole[1]
 
 
 def update_moments(projected, first_old, second_old):
@@ -84,16 +83,6 @@
     return out[:, :width] + (out[:, width : 2 * width] + out[:, 2 * width :])
 
 
-def whole_copies(branch_new, gate_new):
-    mine = jnp.concatenate([branch_new, gate_new], axis=1).astype(jnp.bfloat16)
-    rows, width = mine.shape
-    along_z = from_everyone(mine, Z)
-    along_x = from_everyone(along_z, ("x",))
-    both = from_everyone(along_x, ("c",))
-    whole = both.transpose(2, 1, 0, 3, 4).reshape(-1, width)
-    return whole[:, : width // 2], whole[:, width // 2 :]
-
-
 def local(
     layer_input,
     branch_cotangent,
@@ -108,7 +97,7 @@
     gate_second,
 ):
     rank, width = branch_first.shape
-    factors = whole_factors(branch_factor, gate_factor)
+    factors = in_row_order(gathered(jnp.concatenate([branch_factor, gate_factor], axis=1)))
     rows = jnp.dot(layer_input, factors, preferred_element_type=jnp.float32)
     branch_local = projected_locally(rows[:, :rank], branch_cotangent)
     gate_local = projected_locally(rows[:, rank:], gate_cotangent)
@@ -130,7 +119,10 @@
     gate_step = -step_scale * times_direction(gate_factor, gate_direction)
     branch_new = branch_weight + branch_step
     gate_new = gate_weight + gate_step
-    branch_copy, gate_copy = whole_copies(branch_new, gate_new)
+    copies = in_row_order(
+        gathered(jnp.concatenate([branch_new, gate_new], axis=1).astype(jnp.bfloat16))
+    )
+    branch_copy, gate_copy = copies[:, :width], copies[:, width:]
     return (
         branch_step,
         gate_step,

time: 158 us -> 152 us (0.962); the launches traced: 155 us -> 152 us
  blocking collectives: 135 us -> 109 us
  starting transfers between devices: 3.22 us -> 17.3 us
  other arithmetic: 4.65 us -> 9.06 us
  waiting for transfers between devices: 3.68 us -> 6.26 us
    all_to_all x11 -> x7, blocking collectives: 135 us -> 109 us  [exchanged(): return lax.all_to_all(blocks, axes, split_axis=0, concat_axis=0, tiled=True)]
    ppermute x0 -> x2, starting transfers between devices: none -> 13.1 us  [gathered(): other = lax.ppermute(mine, 'c', [(0, 1), (1, 0)])]
    ppermute x0 -> x2, waiting for transfers between devices: none -> 4.12 us  [gathered(): other = lax.ppermute(mine, 'c', [(0, 1), (1, 0)])]
    another operation x5 -> x7, other arithmetic: 1.29 us -> 3.51 us
  transfers between devices with their start and end apart: 1 -> 3, of which waited for: 1 -> 3; matrix products, arithmetic and copies ran while one was open for 0% -> 1% of each run, Pallas kernels for 0% -> 0%
where the time goes in v2:
time: 152 us
  blocking collectives  109 us (72%)
  starting transfers between devices  17.3 us (11%)
  other arithmetic  9.06 us (6%)
  waiting for transfers between devices  6.26 us (4%)
  local copies, waits for them, and re-layouts  3.97 us (3%)
  matrix products  3.46 us (2%)
  between operations  2.27 us (1%)
    all_to_all x7, blocking collectives, exchanged(): return lax.all_to_all(blocks, axes, split_axis=0, concat_axis=0, tiled=True)  109 us
    ppermute x2, starting transfers between devices, gathered(): other = lax.ppermute(mine, 'c', [(0, 1), (1, 0)])  13.1 us
    all_to_all x1, starting transfers between devices, exchanged(): return lax.all_to_all(blocks, axes, split_axis=0, concat_axis=0, tiled=True)  4.18 us
    ppermute x2, waiting for transfers between devices, gathered(): other = lax.ppermute(mine, 'c', [(0, 1), (1, 0)])  4.12 us
  transfers between devices with their start and end apart: 3, of which 3 were waited for; matrix products, arithmetic and copies ran while one was open for 1% of the time, Pallas kernels for 0%

profile of v2, /device:TPU:1, one launch (start us, length us, event | category | flops | bytes accessed | tf_op | source)
XLA Modules:
  0.0 151.5 jit_solution(10120730310700610420)
XLA Ops:
  0.7 0.9 pad_maximum_fusion.3
  1.5 27.8 %all_to_all.40 = bf16[8,16,256]{2,1,0:T(8,128)(2,1)S(1)} all-to-all(bf16[8,16,256]{2,1,0:T(8,128)(2,1)S(1)} %broadcast_in_dim.18), channel_id=1, replica_groups=mesh['zh'=8,'zl'=2,'x'=4,'c'=2,'tp'=4] {'zh'}, dimensions={0} | all-to-all | bytes 131072 | tf_op jit(solution)/shard_map/all_to_all | solution.py:15
  29.3 11.4 %all_to_all.41 = bf16[8,8,16,256]{3,2,1,0:T(8,128)(2,1)S(1)} all-to-all(bf16[8,8,16,256]{3,2,1,0:T(8,128)(2,1)S(1)} %broadcast_in_dim.19), channel_id=1, replica_groups=mesh['zh'=8,'zl'=2,'x'=4,'c'=2,'tp'=4] {'zl','x'}, dimensions={0} | all-to-all | bytes 1048576 | tf_op jit(solution)/shard_map/all_to_all | solution.py:15
  40.7 0.8 copy.30
  41.6 6.0 %collective-permute-start = (bf16[2,4,8,16,256]{4,3,1,0,2:T(8,128)(2,1)}, bf16[2,4,8,16,256]{4,3,1,0,2:T(8,128)(2,1)}, u32[]{:S(2)}, u32[]{:S(2)}) collective-permute-start(bf16[2,4,8,16,256]{4,3,1,0,2:T(8,128)(2,1)} %bitcast), channel_id=1, source_target_pairs={{0,4},{4,0},{1,5},{5,1},{2,6},{6,2},{3,7},{7,3},{8,12},{12,8},{9,1... | collective-permute-start | bytes 1572872 | tf_op jit(solution)/shard_map/ppermute | solution.py:32
  47.6 1.9 %collective-permute-done = bf16[2,4,8,16,256]{4,3,1,0,2:T(8,128)(2,1)} collective-permute-done((bf16[2,4,8,16,256]{4,3,1,0,2:T(8,128)(2,1)}, bf16[2,4,8,16,256]{4,3,1,0,2:T(8,128)(2,1)}, u32[]{:S(2)}, u32[]{:S(2)}) %collective-permute-start) | collective-permute-done | bytes 524320 | tf_op jit(solution)/shard_map/ppermute | solution.py:32
  49.5 1.3 select_bitcast_fusion.3
  50.9 1.1 convolution_bitcast_fusion
  53.3 10.2 %all_to_all.42 = f32[16,16,256]{2,1,0:T(8,128)S(1)} all-to-all(f32[16,16,256]{2,1,0:T(8,128)S(1)} %bitcast.57), channel_id=1, replica_groups=mesh['zh'=8,'zl'=2,'x'=4,'c'=2,'tp'=4] {'zl','x','c'}, dimensions={0} | all-to-all | bytes 524288 | tf_op jit(solution)/shard_map/all_to_all | solution.py:15
  63.5 15.7 %all_to_all.43 = f32[8,16,256]{2,1,0:T(8,128)S(1)} all-to-all(f32[8,16,256]{2,1,0:T(8,128)S(1)} %broadcast_in_dim.20), channel_id=1, replica_groups=mesh['zh'=8,'zl'=2,'x'=4,'c'=2,'tp'=4] {'zh'}, dimensions={0} | all-to-all | bytes 262144 | tf_op jit(solution)/shard_map/all_to_all | solution.py:15
  79.2 14.2 %all_to_all.44 = f32[16,16,256]{2,1,0:T(8,128)S(1)} all-to-all(f32[16,16,256]{2,1,0:T(8,128)S(1)} %broadcast_in_dim.21), channel_id=1, replica_groups=mesh['zh'=8,'zl'=2,'x'=4,'c'=2,'tp'=4] {'zl','x','c'}, dimensions={0} | all-to-all | bytes 524288 | tf_op jit(solution)/shard_map/all_to_all | solution.py:15
  93.5 1.6 %reduce-precision_convert_fusion.3 = (bf16[128,256]{1,0:T(8,128)(2,1)}, f32[128,256]{1,0:T(8,128)S(1)}, f32[128,256]{1,0:T(8,128)}, f32[128,256]{1,0:T(8,128)}) fusion(f32[8,16,256]{2,1,0:T(8,128)S(1)} %get-tuple-element.34, f32[128,256]{1,0:T(8,128)S(1)} %copy-done.1, f32[128,256]{1,0:T(8,128)} %param.19), kind=kLoop, calls=%fused_computation.39 | loop fusion | flops 327680 | bytes 851968 | tf_op jit(solution)/shard_map/convert_element_type | solution.py:81
  95.8 1.3 multiply_reduce_fusion.1
  99.0 4.2 %all-to-all-start.5 = ((f32[4,1,128]{2,1,0:T(1,128)}), f32[4,1,128]{2,1,0:T(1,128)}, u32[]{:S(2)}, u32[]{:S(2)}) async-start(f32[4,1,128]{2,1,0:T(1,128)} %broadcast_in_dim_broadcast_in_dim.3), calls=%async_computation.5 | async-start | bytes 4096 | tf_op jit(solution)/shard_map/all_to_all | solution.py:15
  103.2 1.0 convolution_bitcast_fusion.1
  104.2 0.8 convolution_bitcast_fusion.2
  105.0 2.1 %all-to-all-done.5 = f32[4,1,128]{2,1,0:T(1,128)} async-done(((f32[4,1,128]{2,1,0:T(1,128)}), f32[4,1,128]{2,1,0:T(1,128)}, u32[]{:S(2)}, u32[]{:S(2)}) %all-to-all-start.5) | async-done | bytes 2080 | tf_op jit(solution)/shard_map/all_to_all | solution.py:15
  107.2 0.7 reduce_sum.51
  108.6 1.3 fusion.36
  109.9 16.2 %all_to_all.45 = bf16[8,16,512]{2,1,0:T(8,128)(2,1)S(1)} all-to-all(bf16[8,16,512]{2,1,0:T(8,128)(2,1)S(1)} %broadcast_in_dim.22), channel_id=1, replica_groups=mesh['zh'=8,'zl'=2,'x'=4,'c'=2,'tp'=4] {'zh'}, dimensions={0} | all-to-all | bytes 262144 | tf_op jit(solution)/shard_map/all_to_all | solution.py:15
  126.3 13.9 %all_to_all.46 = bf16[8,8,16,512]{3,2,1,0:T(8,128)(2,1)S(1)} all-to-all(bf16[8,8,16,512]{3,2,1,0:T(8,128)(2,1)S(1)} %broadcast_in_dim.23), channel_id=1, replica_groups=mesh['zh'=8,'zl'=2,'x'=4,'c'=2,'tp'=4] {'zl','x'}, dimensions={0} | all-to-all | bytes 2097152 | tf_op jit(solution)/shard_map/all_to_all | solution.py:15
  140.2 7.1 %collective-permute-start.1 = (bf16[2,4,8,16,512]{4,3,2,1,0:T(8,128)(2,1)S(1)}, bf16[2,4,8,16,512]{4,3,2,1,0:T(8,128)(2,1)S(1)}, u32[]{:S(2)}, u32[]{:S(2)}) collective-permute-start(bf16[2,4,8,16,512]{4,3,2,1,0:T(8,128)(2,1)S(1)} %bitcast.54), channel_id=1, source_target_pairs={{0,4},{4,0},{1,5},{5,1},{2,6},{6,2},{3,7},{7,3},{8,12},{12,8},{9,1... | collective-permute-start | bytes 3145736 | tf_op jit(solution)/shard_map/ppermute | solution.py:32
  147.2 2.3 %collective-permute-done.1 = bf16[2,4,8,16,512]{4,3,2,1,0:T(8,128)(2,1)S(1)} collective-permute-done((bf16[2,4,8,16,512]{4,3,2,1,0:T(8,128)(2,1)S(1)}, bf16[2,4,8,16,512]{4,3,2,1,0:T(8,128)(2,1)S(1)}, u32[]{:S(2)}, u32[]{:S(2)}) %collective-permute-start.1) | collective-permute-done | bytes 1048608 | tf_op jit(solution)/shard_map/ppermute | solution.py:32
  150.1 1.5 fusion.44
  (37 shorter events, 4.1 us)
Async XLA Ops:
  0.6 50.2 %copy-start = (bf16[768,2048]{1,0:T(8,128)(2,1)S(1)}, bf16[768,2048]{1,0:T(8,128)(2,1)}, u32[]{:S(2)}) copy-start(bf16[768,2048]{1,0:T(8,128)(2,1)} %param.11) | copy-start | bytes 9437188
  41.6 7.9 %collective-permute-start = (bf16[2,4,8,16,256]{4,3,1,0,2:T(8,128)(2,1)}, bf16[2,4,8,16,256]{4,3,1,0,2:T(8,128)(2,1)}, u32[]{:S(2)}, u32[]{:S(2)}) collective-permute-start(bf16[2,4,8,16,256]{4,3,1,0,2:T(8,128)(2,1)} %bitcast), channel_id=1, source_target_pairs={{0,4},{4,0},{1,5},{5,1},{2,6},{6,2},{3,7},{7,3},{8,12},{12,8},{9,1... | collective-permute-start | bytes 1572872 | tf_op jit(solution)/shard_map/ppermute | solution.py:32
  50.8 1.2 copy-start.5
  51.9 1.0 copy-start.6
  53.2 40.2 %copy-start.1 = (f32[128,256]{1,0:T(8,128)S(1)}, f32[128,256]{1,0:T(8,128)}, u32[]{:S(2)}) copy-start(f32[128,256]{1,0:T(8,128)} %param.21) | copy-start | bytes 393220
  63.5 32.3 %copy-start.2 = (f32[128,256]{1,0:T(8,128)S(1)}, f32[128,256]{1,0:T(8,128)}, u32[]{:S(2)}) copy-start(f32[128,256]{1,0:T(8,128)} %param.20) | copy-start | bytes 393220
  79.2 16.6 %copy-start.3 = (f32[128,256]{1,0:T(8,128)S(1)}, f32[128,256]{1,0:T(8,128)}, u32[]{:S(2)}) copy-start(f32[128,256]{1,0:T(8,128)} %param.18) | copy-start | bytes 393220
  79.2 28.7 %copy-start.4 = (f32[16,256]{1,0:T(8,128)S(1)}, f32[16,256]{1,0:T(8,128)}, u32[]{:S(2)}) copy-start(f32[16,256]{1,0:T(8,128)} %param.17) | copy-start | bytes 49156
  99.0 8.2 %all-to-all-start.5 = ((f32[4,1,128]{2,1,0:T(1,128)}), f32[4,1,128]{2,1,0:T(1,128)}, u32[]{:S(2)}, u32[]{:S(2)}) async-start(f32[4,1,128]{2,1,0:T(1,128)} %broadcast_in_dim_broadcast_in_dim.3), calls=%async_computation.5 | async-start | bytes 4096 | tf_op jit(solution)/shard_map/all_to_all | solution.py:15
  140.2 9.3 %collective-permute-start.1 = (bf16[2,4,8,16,512]{4,3,2,1,0:T(8,128)(2,1)S(1)}, bf16[2,4,8,16,512]{4,3,2,1,0:T(8,128)(2,1)S(1)}, u32[]{:S(2)}, u32[]{:S(2)}) collective-permute-start(bf16[2,4,8,16,512]{4,3,2,1,0:T(8,128)(2,1)S(1)} %bitcast.54), channel_id=1, source_target_pairs={{0,4},{4,0},{1,5},{5,1},{2,6},{6,2},{3,7},{7,3},{8,12},{12,8},{9,1... | collective-permute-start | bytes 3145736 | tf_op jit(solution)/shard_map/ppermute | solution.py:32

commit v3 on v2

v3 whole, which is shorter than its diff:
```python
import functools

import jax
import jax.numpy as jnp
from jax import lax
from jax.experimental import pallas as pl
from jax.experimental.pallas import tpu as pltpu
from jax.sharding import Mesh
from jax.sharding import PartitionSpec as P

FS = ("zh", "zl", "x", "c")
FAR = ("zh",)
NEAR = ("zl", "x")
NEAR_CORES = ("zl", "x", "c")

first_decay = 0.8
second_decay = 0.9
learn_rate = 0.5


def size_of(axes):
    peers = 1
    for a in axes:
        peers *= lax.axis_size(a)
    return peers


def exchanged(blocks, axes):
    return lax.all_to_all(blocks, axes, split_axis=0, concat_axis=0, tiled=True)


def from_everyone(x, axes):
    return exchanged(jnp.broadcast_to(x, (size_of(axes), *x.shape)), axes)


def in_row_order(blocks):
    return blocks.transpose(3, 1, 2, 0, 4, 5).reshape(-1, blocks.shape[-1])


def two_parts(x):
    high = lax.reduce_precision(x, 8, 7)
    return high.astype(jnp.bfloat16), (x - high).astype(jnp.bfloat16)


def projected_locally(rows, cotangent):
    high, low = two_parts(rows)
    rank = rows.shape[1]
    both = lax.dot_general(
        jnp.concatenate([high, low], axis=1),
        cotangent,
        (((0,), (0,)), ((), ())),
        preferred_element_type=jnp.float32,
    )
    return both[:rank] + both[rank:]


def moments_kernel(
    projected,
    branch_first,
    gate_first,
    branch_second,
    gate_second,
    branch_first_new,
    gate_first_new,
    branch_second_new,
    gate_second_new,
    parts,
    squares,
):
    rank, width = branch_first.shape
    total = jnp.zeros((8, 128), jnp.float32)
    both = (
        (branch_first, branch_second, branch_first_new, branch_second_new),
        (gate_first, gate_second, gate_first_new, gate_second_new),
    )
    for p, (first, second, first_new, second_new) in enumerate(both):
        r = projected[p]
        moved = first_decay * first[...] + (1.0 - first_decay) * r
        spread = second_decay * second[...] + (1.0 - second_decay) * r * r
        first_new[...] = moved
        second_new[...] = spread
        direction = moved / jnp.sqrt(spread)
        high = direction.astype(jnp.bfloat16)
        rest = direction - high.astype(jnp.float32)
        middle = rest.astype(jnp.bfloat16)
        low = (rest - middle.astype(jnp.float32)).astype(jnp.bfloat16)
        parts[p, :, :width] = high
        parts[p, :, width : 2 * width] = middle
        parts[p, :, 2 * width :] = low
        squared = direction * direction
        for column in range(0, width, 128):
            total += jnp.sum(
                squared[:, column : column + 128].reshape(rank // 8, 8, 128), axis=0
            )
    for peer in range(squares.shape[0]):
        squares[peer] = total


def rows_kernel(
    entries,
    squares,
    parts,
    factors,
    arrived,
    rows_new,
    branch_step,
    gate_step,
    branch_new,
    gate_new,
    steps_all,
):
    block, width = branch_step.shape
    far = factors.shape[0]
    rank = parts.shape[1]
    at = lax.axis_index("zh")
    total = jnp.sum(jnp.sum(squares[...], axis=0), keepdims=True)
    minus_scale = -learn_rate / jnp.sqrt(total / entries + 1e-06)
    steps = (branch_step, gate_step)
    news = (branch_new, gate_new)
    for p in range(2):
        factor = factors[:, :, p * rank : (p + 1) * rank].reshape(far * block, rank)
        out = jnp.dot(factor, parts[p], preferred_element_type=jnp.float32)
        raw = out[:, :width] + (out[:, width : 2 * width] + out[:, 2 * width :])
        step = (minus_scale * raw).reshape(far, block, width)
        weights = arrived[:, (p + 1) * block : (p + 2) * block, :]
        rows_new[:, :, p * width : (p + 1) * width] = (weights + step).astype(jnp.bfloat16)
        steps_all[...] = step
        mine = steps_all[at]
        steps[p][...] = mine
        news[p][...] = arrived[at, (p + 1) * block : (p + 2) * block, :] + mine


def whole():
    return pl.BlockSpec(memory_space=pltpu.VMEM)


def outgoing_kernel(pieces, branch_weight, gate_weight, blocks):
    height = pieces.shape[1]
    block = branch_weight.shape[0]
    piece = jnp.sum(pieces[...], axis=0)
    for peer in range(blocks.shape[0]):
        blocks[peer, :height] = piece
        blocks[peer, height : height + block] = branch_weight[...]
        blocks[peer, height + block :] = gate_weight[...]


def copies_kernel(mine, other, branch_copy, gate_copy):
    near_z, near_x, far, block, _ = mine.shape
    width = branch_copy.shape[1]
    core = lax.axis_index("c")
    for f in range(far):
        for z in range(near_z):
            for x in range(near_x):
                row = ((f * near_z + z) * near_x + x) * 2 * block
                for source, place in ((mine, core), (other, 1 - core)):
                    rows = pl.ds(pl.multiple_of(row + place * block, block), block)
                    branch_copy[rows, :] = source[z, x, f, :, :width]
                    gate_copy[rows, :] = source[z, x, f, :, width:]


def outgoing(pieces, branch_weight, gate_weight, peers):
    height = pieces.shape[1] + 2 * branch_weight.shape[0]
    return pl.pallas_call(
        outgoing_kernel,
        out_shape=jax.ShapeDtypeStruct((peers, height, pieces.shape[2]), jnp.float32),
        in_specs=[whole()] * 3,
        out_specs=whole(),
        compiler_params=pltpu.CompilerParams(vmem_limit_bytes=4 << 20),
        name="outgoing",
    )(pieces, branch_weight, gate_weight)


def whole_copies(mine, other):
    near_z, near_x, far, block, columns = mine.shape
    copy = jax.ShapeDtypeStruct((2 * near_z * near_x * far * block, columns // 2), jnp.bfloat16)
    return pl.pallas_call(
        copies_kernel,
        out_shape=[copy, copy],
        in_specs=[whole()] * 2,
        out_specs=[whole()] * 2,
        compiler_params=pltpu.CompilerParams(vmem_limit_bytes=8 << 20),
        name="whole_copies",
    )(mine, other)


def moments(projected, branch_first, gate_first, branch_second, gate_second, planes):
    rank, width = branch_first.shape
    f32 = jax.ShapeDtypeStruct((rank, width), jnp.float32)
    return pl.pallas_call(
        moments_kernel,
        out_shape=[
            f32,
            f32,
            f32,
            f32,
            jax.ShapeDtypeStruct((2, rank, 3 * width), jnp.bfloat16),
            jax.ShapeDtypeStruct((planes, 8, 128), jnp.float32),
        ],
        in_specs=[whole()] * 5,
        out_specs=[whole()] * 6,
        compiler_params=pltpu.CompilerParams(vmem_limit_bytes=6 << 20),
        name="moments",
    )(projected, branch_first, gate_first, branch_second, gate_second)


def new_rows(entries, squares, parts, factors, arrived, block, width):
    far = factors.shape[0]
    f32 = jax.ShapeDtypeStruct((block, width), jnp.float32)
    return pl.pallas_call(
        functools.partial(rows_kernel, entries),
        out_shape=[jax.ShapeDtypeStruct((far, block, 2 * width), jnp.bfloat16), f32, f32, f32, f32],
        in_specs=[whole()] * 4,
        out_specs=[whole()] * 5,
        scratch_shapes=[pltpu.VMEM((far, block, width), jnp.float32)],
        compiler_params=pltpu.CompilerParams(vmem_limit_bytes=6 << 20),
        name="new_rows",
    )(squares, parts, factors, arrived)


def local(
    layer_input,
    branch_cotangent,
    gate_cotangent,
    branch_factor,
    gate_factor,
    branch_weight,
    gate_weight,
    branch_first,
    gate_first,
    branch_second,
    gate_second,
):
    rank, width = branch_first.shape
    block = branch_weight.shape[0]
    near = (lax.axis_size("zl"), lax.axis_size("x"))

    far_factors = from_everyone(jnp.concatenate([branch_factor, gate_factor], axis=1), FAR)
    near_factors = from_everyone(far_factors, NEAR)
    all_factors = from_everyone(near_factors, ("c",))
    factors = in_row_order(all_factors.reshape(2, *near, *far_factors.shape))

    rows = jnp.dot(layer_input, factors, preferred_element_type=jnp.float32)
    both = jnp.stack(
        [
            projected_locally(rows[:, :rank], branch_cotangent),
            projected_locally(rows[:, rank:], gate_cotangent),
        ]
    )
    pieces = both.reshape(size_of(NEAR_CORES), -1, width)
    height = pieces.shape[1]
    blocks = outgoing(
        exchanged(pieces, NEAR_CORES), branch_weight, gate_weight, size_of(FAR)
    )
    arrived = exchanged(blocks, FAR)
    total = arrived[:, :height].sum(axis=0)
    projected = from_everyone(total, NEAR_CORES).reshape(both.shape)

    planes = lax.axis_size("tp")
    (
        branch_first_new,
        gate_first_new,
        branch_second_new,
        gate_second_new,
        parts,
        squares,
    ) = moments(projected, branch_first, gate_first, branch_second, gate_second, planes)
    squares = exchanged(squares, ("tp",))
    rows_new, branch_step, gate_step, branch_new, gate_new = new_rows(
        2 * rank * width * planes,
        squares,
        parts,
        far_factors,
        arrived,
        block,
        width,
    )

    mine = from_everyone(rows_new, NEAR).reshape(*near, *rows_new.shape)
    other = lax.ppermute(mine, "c", [(0, 1), (1, 0)])
    branch_copy, gate_copy = whole_copies(mine, other)
    return (
        branch_step,
        gate_step,
        branch_new,
        gate_new,
        branch_copy,
        gate_copy,
        branch_first_new,
        gate_first_new,
        branch_second_new,
        gate_second_new,
    )


def solution(mesh):
    finer = Mesh(
        mesh.devices.reshape(8, 2, 4, 2, mesh.shape["tp"]), ("zh", "zl", "x", "c", "tp")
    )
    sharded = P(FS, None)
    split = P(FS, "tp")
    kept = P(None, "tp")
    in_specs = (sharded, split, split, sharded, sharded, split, split, kept, kept, kept, kept)
    out_specs = (split, split, split, split, kept, kept, kept, kept, kept, kept)
    return jax.shard_map(local, mesh=finer, in_specs=in_specs, out_specs=out_specs, check_vma=False)
```

time: 152 us -> 137 us (0.901)
  blocking collectives: 109 us -> 121 us
  starting transfers between devices: 17.3 us -> 5.62 us
  other arithmetic: 9.06 us -> 1.02 us
  waiting for transfers between devices: 6.26 us -> 2.26 us
  local copies, waits for them, and re-layouts: 3.97 us -> 0.5 us
  Pallas kernels: 0 us -> 3.3 us
  matrix products: 3.46 us -> 1.62 us
    all_to_all x7 -> x8, blocking collectives: 109 us -> 121 us  [exchanged(): return lax.all_to_all(blocks, axes, split_axis=0, concat_axis=0, tiled=True)]
    ppermute x2 -> x1, starting transfers between devices: 13.1 us -> 5.62 us  [local(): other = lax.ppermute(mine, 'c', [(0, 1), (1, 0)])]
    all_to_all x1 -> x0, starting transfers between devices: 4.18 us -> none  [exchanged(): return lax.all_to_all(blocks, axes, split_axis=0, concat_axis=0, tiled=True)]
    another operation x7 -> x2, other arithmetic: 3.51 us -> 0.05 us  [local(): jnp.stack([projected_locally(rows[:, :rank], branch_cotangent), projected...]
    pallas_call x0 -> x4, Pallas kernels: none -> 3.3 us  [the longest x1 1.49 us: whole_copies(): pl.pallas_call(copies_kernel, out_shape=[copy, copy], in_specs=[whole()]...]
    convert_element_type x3 -> x0, other arithmetic: 2.31 us -> none  [times_direction(): p.astype(jnp.bfloat16)]
    all_to_all x1 -> x0, waiting for transfers between devices: 2.14 us -> none  [exchanged(): return lax.all_to_all(blocks, axes, split_axis=0, concat_axis=0, tiled=True)]
    reduce_sum x4 -> x1, other arithmetic: 2.08 us -> 0.01 us  [local(): total = arrived[:, :height].sum(axis=0)]
  transfers between devices with their start and end apart: 3 -> 1, of which waited for: 3 -> 1; matrix products, arithmetic and copies ran while one was open for 1% -> 0% of each run, Pallas kernels for 0% -> 0%
where the time goes in v3:
time: 137 us
  blocking collectives  121 us (88%)
  starting transfers between devices  5.62 us (4%)
  Pallas kernels  3.3 us (2%)
  waiting for transfers between devices  2.26 us (2%)
  matrix products  1.62 us (1%)
    all_to_all x8, blocking collectives, exchanged(): return lax.all_to_all(blocks, axes, split_axis=0, concat_axis=0, tiled=True)  121 us
    ppermute x1, starting transfers between devices, local(): other = lax.ppermute(mine, 'c', [(0, 1), (1, 0)])  5.62 us
  transfers between devices with their start and end apart: 1, of which 1 were waited for; matrix products, arithmetic and copies ran while one was open for 0% of the time, Pallas kernels for 0%

profile of v3, /device:TPU:1, one launch (start us, length us, event | category | flops | bytes accessed | tf_op | source)
XLA Modules:
  0.0 136.5 jit_solution(16670188081238257614)
XLA Ops:
  0.6 0.0 copy-start
  0.7 0.9 pad_maximum_fusion.1
  1.5 27.8 %all_to_all.40.factors = bf16[8,16,256]{2,1,0:T(8,128)(2,1)S(1)} all-to-all(bf16[8,16,256]{2,1,0:T(8,128)(2,1)S(1)} %broadcast_in_dim.15), channel_id=1, replica_groups=mesh['zh'=8,'zl'=2,'x'=4,'c'=2,'tp'=4] {'zh'}, dimensions={0} | all-to-all | bytes 131072 | tf_op jit(solution)/shard_map/all_to_all | solution.py:29
  29.3 11.4 %all_to_all.41 = bf16[8,8,16,256]{3,2,1,0:T(8,128)(2,1)S(1)} all-to-all(bf16[8,8,16,256]{3,2,1,0:T(8,128)(2,1)S(1)} %broadcast_in_dim.16), channel_id=1, replica_groups=mesh['zh'=8,'zl'=2,'x'=4,'c'=2,'tp'=4] {'zl','x'}, dimensions={0} | all-to-all | bytes 1048576 | tf_op jit(solution)/shard_map/all_to_all | solution.py:29
  40.8 0.1 broadcast_in_dim.17
  40.9 8.3 %all_to_all.42 = bf16[2,8,8,16,256]{4,3,1,2,0:T(8,128)(2,1)S(1)} all-to-all(bf16[2,8,8,16,256]{4,3,1,2,0:T(8,128)(2,1)S(1)} %broadcast_in_dim.17), channel_id=1, replica_groups=mesh['zh'=8,'zl'=2,'x'=4,'c'=2,'tp'=4] {'c'}, dimensions={0} | all-to-all | bytes 2097152 | tf_op jit(solution)/shard_map/all_to_all | solution.py:29
  49.2 0.1 copy.22
  49.4 0.0 copy-start.7
  49.4 1.1 convolution_bitcast_fusion
  50.5 0.0 copy-start.5
  50.5 0.1 reduce-precision_convert_fusion.1
  50.7 0.3 fusion.2
  50.9 0.3 fusion.6
  51.3 10.2 %all_to_all.43.pieces = f32[16,16,256]{2,1,0:T(8,128)S(1)} all-to-all(f32[16,16,256]{2,1,0:T(8,128)S(1)} %bitcast.22), channel_id=1, replica_groups=mesh['zh'=8,'zl'=2,'x'=4,'c'=2,'tp'=4] {'zl','x','c'}, dimensions={0} | all-to-all | bytes 524288 | tf_op jit(solution)/shard_map/all_to_all | solution.py:29
  61.5 25.4 %all_to_all.44.arrived = f32[8,48,256]{2,1,0:T(8,128)S(1)} all-to-all(f32[8,48,256]{2,1,0:T(8,128)S(1)} %outgoing.1), channel_id=1, replica_groups=mesh['zh'=8,'zl'=2,'x'=4,'c'=2,'tp'=4] {'zh'}, dimensions={0} | all-to-all | bytes 786432 | tf_op jit(solution)/shard_map/all_to_all | solution.py:29
  86.9 14.6 %all_to_all.45 = f32[16,16,256]{2,1,0:T(8,128)S(1)} all-to-all(f32[16,16,256]{2,1,0:T(8,128)S(1)} %broadcast_in_dim.18), channel_id=1, replica_groups=mesh['zh'=8,'zl'=2,'x'=4,'c'=2,'tp'=4] {'zl','x','c'}, dimensions={0} | all-to-all | bytes 524288 | tf_op jit(solution)/shard_map/all_to_all | solution.py:29
  101.5 0.9 moments.1
  102.4 8.2 %all_to_all.46.squares = f32[4,8,128]{2,1,0:T(8,128)S(1)} all-to-all(f32[4,8,128]{2,1,0:T(8,128)S(1)} %get-tuple-element.23), channel_id=1, replica_groups=mesh['zh'=8,'zl'=2,'x'=4,'c'=2,'tp'=4] {'tp'}, dimensions={0} | all-to-all | bytes 32768 | tf_op jit(solution)/shard_map/all_to_all | solution.py:29
  110.6 0.9 new_rows.1
  111.5 0.1 broadcast_in_dim.19
  111.6 15.5 %all_to_all.47 = bf16[8,8,16,512]{3,2,1,0:T(8,128)(2,1)S(1)} all-to-all(bf16[8,8,16,512]{3,2,1,0:T(8,128)(2,1)S(1)} %broadcast_in_dim.19), channel_id=1, replica_groups=mesh['zh'=8,'zl'=2,'x'=4,'c'=2,'tp'=4] {'zl','x'}, dimensions={0} | all-to-all | bytes 2097152 | tf_op jit(solution)/shard_map/all_to_all | solution.py:29
  127.2 5.6 %collective-permute-start = (bf16[2,4,8,16,512]{4,3,2,1,0:T(8,128)(2,1)S(1)}, bf16[2,4,8,16,512]{4,3,2,1,0:T(8,128)(2,1)S(1)}, u32[]{:S(2)}, u32[]{:S(2)}) collective-permute-start(bf16[2,4,8,16,512]{4,3,2,1,0:T(8,128)(2,1)S(1)} %bitcast.18), channel_id=1, source_target_pairs={{0,4},{4,0},{1,5},{5,1},{2,6},{6,2},{3,7},{7,3},{8,12},{12,8},{9,1... | collective-permute-start | bytes 3145736 | tf_op jit(solution)/shard_map/ppermute | solution.py:279
  132.8 2.3 %collective-permute-done.other = bf16[2,4,8,16,512]{4,3,2,1,0:T(8,128)(2,1)S(1)} collective-permute-done((bf16[2,4,8,16,512]{4,3,2,1,0:T(8,128)(2,1)S(1)}, bf16[2,4,8,16,512]{4,3,2,1,0:T(8,128)(2,1)S(1)}, u32[]{:S(2)}, u32[]{:S(2)}) %collective-permute-start) | collective-permute-done | bytes 1048608 | tf_op jit(solution)/shard_map/ppermute | solution.py:279
  135.0 1.5 %whole_copies.1 = (bf16[2048,256]{1,0:T(8,128)(2,1)}, bf16[2048,256]{1,0:T(8,128)(2,1)}) custom-call(bf16[2,4,8,16,512]{4,3,2,1,0:T(8,128)(2,1)S(1)} %bitcast.19, bf16[2,4,8,16,512]{4,3,2,1,0:T(8,128)(2,1)S(1)} %collective-permute-done.other), custom_call_target="tpu_custom_call" | custom-call | tf_op jit(solution)/shard_map/whole_copies/pallas_call | solution.py:176
  (23 shorter events, 0.2 us)
Async XLA Ops:
  0.6 48.7 %copy-start = (bf16[768,2048]{1,0:T(8,128)(2,1)S(1)}, bf16[768,2048]{1,0:T(8,128)(2,1)}, u32[]{:S(2)}) copy-start(bf16[768,2048]{1,0:T(8,128)(2,1)} %param.11) | copy-start | bytes 9437188
  49.4 1.2 copy-start.7
  49.4 1.6 %copy-start.8 = (bf16[768,256]{1,0:T(8,128)(2,1)S(1)}, bf16[768,256]{1,0:T(8,128)(2,1)}, u32[]{:S(2)}) copy-start(bf16[768,256]{1,0:T(8,128)(2,1)} %param.13) | copy-start | bytes 1179652
  50.5 11.0 %copy-start.5 = (f32[16,256]{1,0:T(8,128)S(1)}, f32[16,256]{1,0:T(8,128)}, u32[]{:S(2)}) copy-start(f32[16,256]{1,0:T(8,128)} %branch_weight.1) | copy-start | bytes 49156
  50.5 11.0 %copy-start.6 = (f32[16,256]{1,0:T(8,128)S(1)}, f32[16,256]{1,0:T(8,128)}, u32[]{:S(2)}) copy-start(f32[16,256]{1,0:T(8,128)} %gate_weight.1) | copy-start | bytes 49156
  50.6 50.9 %copy-start.1 = (f32[128,256]{1,0:T(8,128)S(1)}, f32[128,256]{1,0:T(8,128)}, u32[]{:S(2)}) copy-start(f32[128,256]{1,0:T(8,128)} %branch_first.1) | copy-start | bytes 393220
  50.6 50.9 %copy-start.2 = (f32[128,256]{1,0:T(8,128)S(1)}, f32[128,256]{1,0:T(8,128)}, u32[]{:S(2)}) copy-start(f32[128,256]{1,0:T(8,128)} %gate_first.1) | copy-start | bytes 393220
  50.6 50.9 %copy-start.3 = (f32[128,256]{1,0:T(8,128)S(1)}, f32[128,256]{1,0:T(8,128)}, u32[]{:S(2)}) copy-start(f32[128,256]{1,0:T(8,128)} %branch_second.1) | copy-start | bytes 393220
  50.6 50.9 %copy-start.4 = (f32[128,256]{1,0:T(8,128)S(1)}, f32[128,256]{1,0:T(8,128)}, u32[]{:S(2)}) copy-start(f32[128,256]{1,0:T(8,128)} %gate_second.1) | copy-start | bytes 393220
  127.2 7.9 %collective-permute-start = (bf16[2,4,8,16,512]{4,3,2,1,0:T(8,128)(2,1)S(1)}, bf16[2,4,8,16,512]{4,3,2,1,0:T(8,128)(2,1)S(1)}, u32[]{:S(2)}, u32[]{:S(2)}) collective-permute-start(bf16[2,4,8,16,512]{4,3,2,1,0:T(8,128)(2,1)S(1)} %bitcast.18), channel_id=1, source_target_pairs={{0,4},{4,0},{1,5},{5,1},{2,6},{6,2},{3,7},{7,3},{8,12},{12,8},{9,1... | collective-permute-start | bytes 3145736 | tf_op jit(solution)/shard_map/ppermute | solution.py:279
